TPU v7x, 32 devices: a whole 2x2x4 slice. The times are simulated.
32 devices in a mesh: grp: 2 (over y), sp: 4 (over z), tp: 4 (over x, core).
Axes of the slice: x: 2, y: 2, z: 4, core: 2. Of those that a mesh axis runs over, the one named last changes fastest.
Arguments:
- target: bfloat16 [2048, 2048], P(('grp', 'sp', 'tp')), parts along dimension 0, may hold values from -20 to 20
- source: bfloat16 [4096, 2048], P(('grp', 'sp')), parts along dimension 0, may hold values from -20 to 20
- source_gain: float32 [2048], replicated, may hold values from 0.1 to 1.9
- query_gain: float32 [2, 2048], replicated, may hold values from 0.1 to 1.9
- out_gain: float32 [2, 2048], replicated, may hold values from 0.1 to 1.9
- query_weight: bfloat16 [2, 2048, 2048], P(None, None, 'tp'), may hold values from -1 to 1
- key_weight: bfloat16 [2, 2048, 512], P(None, None, 'tp'), may hold values from -1 to 1
- value_weight: bfloat16 [2, 2048, 512], P(None, None, 'tp'), may hold values from -0.125 to 0.125
- out_weight: bfloat16 [2, 2048, 2048], P(None, 'tp'), may hold values from -0.125 to 0.125
Outputs:
- result: bfloat16 [2048, 2048], P(('grp', 'sp', 'tp')), parts along dimension 0
There are 2 independent parts, one for each index of `grp`. A program takes and returns all parts, laid end to end along the dimension named above; an argument that names none is the same for every part. Nothing has to cross between parts.
All inputs are finite; a program needn't handle non-finite values.
Results may differ from a plain program's by a relative error of at most 0.024.
Values may be sent and summed in bfloat16 or wider, within the bound.
A program may use at most 64 MiB of HBM per device.

v0:
```python
import jax
import jax.numpy as jnp
from jax import lax
from jax.sharding import PartitionSpec as P

HD = 256
QH = 8
KVH = 2
LAYERS = 2
EPSILON = 1e-06


def swapped(value, axis, distance):
    mask = 2**distance
    pairs = [(source, source ^ mask) for source in range(lax.axis_size(axis))]
    return lax.ppermute(value, axis, pairs)


def rms_scaled(matrix_rows, gain_row):
    values = matrix_rows.astype(jnp.float32)
    inverse = lax.rsqrt(jnp.mean(values * values, axis=-1, keepdims=True) + EPSILON)
    return values * inverse * gain_row


def group_rounds(holding, bit_count, position):
    for bit_number in range(bit_count):
        my_bit = position >> bit_number & 1
        if holding.shape[0] > 1:
            halves = holding.reshape((holding.shape[0] // 2, 2) + holding.shape[1:])
            kept_part = lax.dynamic_index_in_dim(halves, my_bit, 1, False)
            outgoing = lax.dynamic_index_in_dim(halves, 1 - my_bit, 1, False)
        else:
            kept_part = holding
            outgoing = holding
        arrived = swapped(outgoing, "tp", bit_number)
        holding = jnp.where(
            my_bit == 0,
            jnp.concatenate([kept_part, arrived], 1),
            jnp.concatenate([arrived, kept_part], 1),
        )
    return holding


def spread_heads(factor, piece_index, piece_width):
    columns = jnp.repeat(factor, HD, axis=1)
    pieces = columns.reshape(factor.shape[0], columns.shape[1] // piece_width, piece_width)
    return jnp.take(pieces, piece_index, axis=1)


def merge_partials(weighted, row_peak, row_total, bit_count, position):
    piece_width = weighted.shape[2]
    piece_index = jnp.arange(weighted.shape[1], dtype=jnp.int32)
    for bit_number in range(bit_count):
        my_bit = position >> bit_number & 1
        halves = weighted.reshape(weighted.shape[0], weighted.shape[1] // 2, 2, piece_width)
        kept_part = lax.dynamic_index_in_dim(halves, my_bit, 2, False)
        outgoing = lax.dynamic_index_in_dim(halves, 1 - my_bit, 2, False)
        piece_index = lax.dynamic_index_in_dim(piece_index.reshape(-1, 2), my_bit, 1, False)
        far_weighted, far_peak, far_total = (
            swapped(outgoing.astype(jnp.bfloat16), "tp", bit_number).astype(outgoing.dtype),
            swapped(row_peak.astype(jnp.bfloat16), "tp", bit_number).astype(row_peak.dtype),
            swapped(row_total.astype(jnp.bfloat16), "tp", bit_number).astype(row_total.dtype),
        )
        new_peak = jnp.maximum(row_peak, far_peak)
        near_factor = jnp.exp(row_peak - new_peak)
        far_factor = jnp.exp(far_peak - new_peak)
        row_total = row_total * near_factor + far_total * far_factor
        weighted = kept_part * spread_heads(
            near_factor, piece_index, piece_width
        ) + far_weighted * spread_heads(far_factor, piece_index, piece_width)
        row_peak = new_peak
    return (weighted, row_total, piece_index)


def attend(carried, key_rows, value_rows, grouped, score_scale):
    row_peak, row_total, weighted = carried
    scores = (
        jnp.einsum("rhd,nd->rhn", grouped, key_rows, preferred_element_type=jnp.float32)
        * score_scale
    )
    new_peak = jnp.maximum(row_peak, jnp.max(scores, axis=2))
    weights = jnp.exp(scores - new_peak[:, :, None])
    row_total = jnp.sum(weights, axis=2)
    weighted = jnp.einsum(
        "rhn,nd->rhd", weights.astype(jnp.bfloat16), value_rows, preferred_element_type=jnp.float32
    )
    return (new_peak, row_total, weighted)


def body(
    target,
    source,
    source_gain,
    query_gain,
    out_gain,
    query_weight,
    key_weight,
    value_weight,
    out_weight,
):
    tp_devices = lax.axis_size("tp")
    group_size = tp_devices // KVH
    bit_count = group_size.bit_length() - 1
    position = lax.axis_index("tp") % group_size
    score_scale = HD ** (-0.5)
    heads_here = QH // KVH
    matrices = 2 * LAYERS
    slices = key_weight.shape[2]
    block_rows = source.shape[0] // group_size
    normed_source = rms_scaled(source, source_gain).astype(jnp.bfloat16)
    joined = jnp.concatenate(
        [
            matrix[layer_index]
            for layer_index in range(LAYERS)
            for matrix in (key_weight, value_weight)
        ],
        axis=1,
    )
    key_slices = jnp.dot(normed_source, joined, preferred_element_type=jnp.float32).astype(
        jnp.bfloat16
    )
    holding = group_rounds(
        key_slices.reshape(group_size, 1, block_rows, matrices, slices), bit_count, position
    )
    local_keys = jnp.transpose(holding[0], (2, 1, 0, 3)).reshape(matrices, block_rows, HD)
    residual = target
    stored = None
    for layer_index in range(LAYERS):
        normed = rms_scaled(residual, query_gain[layer_index]).astype(jnp.bfloat16)
        layer_weight = query_weight[layer_index]
        queries = jnp.dot(
            lax.all_gather(normed, "tp", axis=0, tiled=True),
            layer_weight,
            preferred_element_type=jnp.float32,
        ).astype(jnp.bfloat16)
        rows_all = queries.shape[0]
        gathered = group_rounds(queries[None, None], bit_count, position)[0]
        grouped = jnp.transpose(gathered, (1, 0, 2)).reshape(rows_all, heads_here, HD)
        start_state = (
            jnp.full((rows_all, heads_here), -1e30, jnp.float32),
            jnp.zeros((rows_all, heads_here), jnp.float32),
            jnp.zeros((rows_all, heads_here, HD), jnp.float32),
        )
        if layer_index == 0:
            empty_rows = jnp.zeros(
                (lax.axis_size("sp") * block_rows, matrices - 2, HD), jnp.bfloat16
            )
            later_keys = jnp.transpose(local_keys[2:], (1, 0, 2))
            updated = attend(
                (start_state + (empty_rows,))[:3],
                lax.all_gather(local_keys[0], "sp", axis=0, tiled=True),
                lax.all_gather(local_keys[1], "sp", axis=0, tiled=True),
                grouped,
                score_scale,
            )
            kept_rows = lax.all_gather(later_keys, "sp", axis=0, tiled=True)
            row_peak, row_total, weighted, stored = updated + (kept_rows,)
        else:
            row_peak, row_total, weighted = attend(
                start_state,
                stored[:, 2 * layer_index - 2],
                stored[:, 2 * layer_index - 1],
                grouped,
                score_scale,
            )
        piece_width = heads_here * HD // group_size
        merged, row_total, piece_index = merge_partials(
            weighted.reshape(rows_all, group_size, piece_width),
            row_peak,
            row_total,
            bit_count,
            position,
        )
        attended = (merged[:, 0] / spread_heads(row_total, piece_index, piece_width)[:, 0]).astype(
            jnp.bfloat16
        )
        out_layer = out_weight[layer_index]
        summed_rows = lax.psum_scatter(
            jnp.dot(attended, out_layer, preferred_element_type=jnp.float32).astype(jnp.bfloat16),
            "tp",
            scatter_dimension=0,
            tiled=True,
        ).astype(jnp.float32)
        residual = (
            residual.astype(jnp.float32) + rms_scaled(summed_rows, out_gain[layer_index])
        ).astype(jnp.bfloat16)
    return residual


def solution(mesh):
    in_specs = (
        P(("grp", "sp", "tp"), None),
        P(("grp", "sp"), None),
        P(),
        P(),
        P(),
        P(None, None, "tp"),
        P(None, None, "tp"),
        P(None, None, "tp"),
        P(None, "tp", None),
    )
    out_specs = P(("grp", "sp", "tp"), None)
    return jax.shard_map(body, mesh=mesh, in_specs=in_specs, out_specs=out_specs, check_vma=False)
```

profile of v0, /device:TPU:0, one launch (start us, length us, event | category | flops | bytes accessed | tf_op | source)
XLA Modules:
  0.0 189.7 jit_solution(303224144333175223)
XLA Ops:
  7.4 1.1 fusion.51
  8.6 1.8 fusion.53
  10.4 2.7 %slice_bitcast_fusion.6 = (bf16[2048,128]{1,0:T(8,128)(2,1)S(1)}, bf16[2048,128]{1,0:T(8,128)(2,1)}, bf16[2048,128]{1,0:T(8,128)(2,1)}, bf16[2048,128]{1,0:T(8,128)(2,1)}) fusion(bf16[2,2048,128]{2,1,0:T(8,128)(2,1)} %param.18, bf16[2,2048,128]{2,1,0:T(8,128)(2,1)} %param.17), kind=kLoop, calls=%fused_computation.92 | loop fusion | bytes 4194304 | tf_op jit(solution)/shard_map/squeeze | solution.py:113
  13.7 2.7 %fusion.36 = bf16[512,512]{1,0:T(8,128)(2,1)S(1)} fusion(bf16[2048,128]{1,0:T(8,128)(2,1)} %get-tuple-element.28, bf16[2048,128]{1,0:T(8,128)(2,1)} %get-tuple-element.41, bf16[2048,128]{1,0:T(8,128)(2,1)S(1)} %get-tuple-element.27, bf16[2048,128]{1,0:T(8,128)(2,1)} %get-tuple-element.42, bf16[512,2048]{1,0:T(8,128)(2,1)S(1)} %copy-done.1, ...), kind=kOutput, calls=%fused_computation.41 | convolution fusion | flops 1086586880 | bytes 4728832 | tf_op jit(solution)/shard_map/dot_general | solution.py:119
  17.3 1.1 collective-permute-done.1
  18.7 11.2 %all-gather.4.cloned.1.call-done = bf16[256,2048]{1,0:T(8,128)(2,1)} async-done(((bf16[64,2048]{1,0:T(8,128)(2,1)}), bf16[256,2048]{1,0:T(8,128)(2,1)}) %all-gather.4.cloned.1.call-update) | async-done | bytes 1048592 | tf_op jit(solution)/shard_map/all_gather | solution.py:132
  30.0 2.6 %fusion.41 = bf16[256,512]{1,0:T(8,128)(2,1)S(1)} fusion(bf16[256,2048]{1,0:T(8,128)(2,1)} %all-gather.4.cloned.1.call-done, bf16[2,2048,512]{2,1,0:T(8,128)(2,1)} %param.16), kind=kOutput, calls=%fused_computation.42 | convolution fusion | flops 537001984 | bytes 3407872 | tf_op jit(solution)/shard_map/dot_general | solution.py:131
  32.9 16.0 %all_gather.16 = bf16[1024,256]{1,0:T(8,128)(2,1)S(1)} all-gather(bf16[256,256]{1,0:T(8,128)(2,1)S(1)} %bitcast.151), channel_id=1, replica_groups=mesh['grp'=2,'sp'=4,'tp'=4] {'sp'}, dimensions={0}, use_global_device_ids=true | all-gather | bytes 655360 | tf_op jit(solution)/shard_map/all_gather | solution.py:151
  49.0 16.1 %all_gather.17 = bf16[1024,256]{0,1:T(8,128)(2,1)S(1)} all-gather(bf16[256,256]{0,1:T(8,128)(2,1)S(1)} %bitcast.152), channel_id=1, replica_groups=mesh['grp'=2,'sp'=4,'tp'=4] {'sp'}, dimensions={0}, use_global_device_ids=true | all-gather | bytes 655360 | tf_op jit(solution)/shard_map/all_gather | solution.py:152
  67.2 1.0 fusion.9
  71.7 1.9 convolution_convert_fusion.1
  73.7 24.6 %reduce-scatter.3.cloned.1.call-done = bf16[64,2048]{1,0:T(8,128)(2,1)} async-done(((bf16[256,2048]{1,0:T(8,128)(2,1)}), bf16[64,2048]{1,0:T(8,128)(2,1)}) %reduce-scatter.3.cloned.1.call-update) | async-done | bytes 262160 | tf_op jit(solution)/shard_map/reduce_scatter | solution.py:178
  98.3 1.1 fusion.47
  99.5 1.2 fusion.55
  102.7 15.8 %all-gather.6.cloned.1.call-done = bf16[256,2048]{1,0:T(8,128)(2,1)} async-done(((bf16[64,2048]{1,0:T(8,128)(2,1)}), bf16[256,2048]{1,0:T(8,128)(2,1)}) %all-gather.6.cloned.1.call-update) | async-done | bytes 1048592 | tf_op jit(solution)/shard_map/all_gather | solution.py:132
  118.5 2.6 %fusion.44 = bf16[256,512]{1,0:T(8,128)(2,1)S(1)} fusion(bf16[256,2048]{1,0:T(8,128)(2,1)} %all-gather.6.cloned.1.call-done, bf16[2,2048,512]{2,1,0:T(8,128)(2,1)} %param.16), kind=kOutput, calls=%fused_computation.43 | convolution fusion | flops 537001984 | bytes 3407872 | tf_op jit(solution)/shard_map/dot_general | solution.py:131
  121.4 1.3 collective-permute-done.5
  123.0 24.9 %all-gather.8.cloned.1.call-done = bf16[1024,2,256]{2,0,1:T(8,128)(2,1)} async-done(((bf16[256,2,256]{2,0,1:T(8,128)(2,1)}), bf16[1024,2,256]{2,0,1:T(8,128)(2,1)}) %all-gather.8.cloned.1.call-update) | async-done | bytes 1048592 | tf_op jit(solution)/shard_map/all_gather | solution.py:156
  147.9 2.0 %multiply_reduce_fusion = (f32[256,4]{0,1:T(4,128)S(1)}, f32[256,4,1024]{2,0,1:T(8,128)S(1)}) fusion(bf16[256,4,256]{0,2,1:T(8,128)(2,1)S(1)} %bitcast.138, bf16[1024,2,256]{2,0,1:T(8,128)(2,1)} %all-gather.8.cloned.1.call-done), kind=kOutput, calls=%fused_computation.7 | convolution fusion | flops 538967040 | bytes 5246976 | tf_op jit(solution)/shard_map/rhd,nd->rhn/dot_general | solution.py:78
  150.8 1.1 fusion.7
  154.0 1.8 convolution_convert_fusion
  155.9 24.3 %reduce-scatter.5.cloned.1.call-done = bf16[64,2048]{1,0:T(8,128)(2,1)} async-done(((bf16[256,2048]{1,0:T(8,128)(2,1)}), bf16[64,2048]{1,0:T(8,128)(2,1)}) %reduce-scatter.5.cloned.1.call-update) | async-done | bytes 262160 | tf_op jit(solution)/shard_map/reduce_scatter | solution.py:178
  180.2 1.1 fusion.49
  181.3 1.8 fusion.58
  (84 shorter events, 12.1 us)
Async XLA Ops:
  6.5 6.6 %copy-start.1 = (bf16[512,2048]{1,0:T(8,128)(2,1)S(1)}, bf16[512,2048]{1,0:T(8,128)(2,1)}, u32[]{:S(2)}) copy-start(bf16[512,2048]{1,0:T(8,128)(2,1)} %param.12) | copy-start | bytes 6291460
  6.5 7.1 %copy-start.6 = (f32[2048]{0:T(1024)S(1)}, f32[2048]{0:T(1024)}, u32[]{:S(2)}) copy-start(f32[2048]{0:T(1024)} %param.13) | copy-start | bytes 24580
  6.5 23.4 %all-gather.4.cloned.1.call-start = ((), (), s32[]{:S(2)}) async-start(), calls=%async_computation.2 | async-start | bytes 1310720 | tf_op jit(solution)/shard_map/all_gather | solution.py:132
  10.4 88.0 %reduce-scatter.3.cloned.1.call-start = ((), (), s32[]{:S(2)}) async-start(), calls=%async_computation.3 | async-start | bytes 1310720 | tf_op jit(solution)/shard_map/reduce_scatter | solution.py:178
  16.7 1.7 collective-permute-start.1
  32.6 32.5 %collective-permute-start = (bf16[1,1,256,512]{3,2,1,0:T(8,128)(2,1)S(1)}, bf16[1,1,256,512]{3,2,1,0:T(8,128)(2,1)S(1)}, u32[]{:S(2)}, u32[]{:S(2)}) collective-permute-start(bf16[1,1,256,512]{3,2,1,0:T(8,128)(2,1)S(1)} %bitcast.155), channel_id=1, source_target_pairs={{0,1},{1,0},{2,3},{3,2},{4,5},{5,4},{6,7},{7,6},{8,9},{9,8},{10,11... | collective-permute-start | bytes 786440 | tf_op jit(solution)/shard_map/ppermute | solution.py:16
  67.2 4.6 %copy-start.4 = (bf16[2,512,2048]{2,1,0:T(8,128)(2,1)S(1)}, bf16[2,512,2048]{2,1,0:T(8,128)(2,1)}, u32[]{:S(2)}) copy-start(bf16[2,512,2048]{2,1,0:T(8,128)(2,1)} %param.19) | copy-start | bytes 12582916
  68.2 3.3 %collective-permute-start.3 = (bf16[256,1,512]{0,2,1:T(8,128)(2,1)S(1)}, bf16[256,1,512]{0,2,1:T(8,128)(2,1)S(1)}, u32[]{:S(2)}, u32[]{:S(2)}) collective-permute-start(bf16[256,1,512]{0,2,1:T(8,128)(2,1)S(1)} %fusion.72), channel_id=1, source_target_pairs={{0,1},{1,0},{2,3},{3,2},{4,5},{5,4},{6,7},{7,6},{8,9},{9,8},{10,11... | collective-permute-start | bytes 786440 | tf_op jit(solution)/shard_map/ppermute | solution.py:16
  68.3 3.1 %collective-permute-start.4 = (bf16[256,4]{0,1:T(4,128)(2,1)S(1)}, bf16[256,4]{0,1:T(4,128)(2,1)S(1)}, u32[]{:S(2)}, u32[]{:S(2)}) collective-permute-start(bf16[256,4]{0,1:T(4,128)(2,1)S(1)} %convert_element_type.135), channel_id=1, source_target_pairs={{0,1},{1,0},{2,3},{3,2},{4,5},{5,4},{6,7},{7,6},{8,9},{9,8},{10,11... | collective-permute-start | bytes 6152 | tf_op jit(solution)/shard_map/ppermute | solution.py:16
  68.8 2.6 %collective-permute-start.2 = (bf16[256,4]{0,1:T(4,128)(2,1)S(1)}, bf16[256,4]{0,1:T(4,128)(2,1)S(1)}, u32[]{:S(2)}, u32[]{:S(2)}) collective-permute-start(bf16[256,4]{0,1:T(4,128)(2,1)S(1)} %fusion.91), channel_id=1, source_target_pairs={{0,1},{1,0},{2,3},{3,2},{4,5},{5,4},{6,7},{7,6},{8,9},{9,8},{10,11... | collective-permute-start | bytes 6152 | tf_op jit(solution)/shard_map/ppermute | solution.py:16
  71.6 2.0 %copy-start.3 = (f32[2,2048]{1,0:T(2,128)S(1)}, f32[2,2048]{1,0:T(2,128)}, u32[]{:S(2)}) copy-start(f32[2,2048]{1,0:T(2,128)} %param.15) | copy-start | bytes 49156
  71.6 27.8 %copy-start = (bf16[64,2048]{1,0:T(8,128)(2,1)S(1)}, bf16[64,2048]{1,0:T(8,128)(2,1)}, u32[]{:S(2)}) copy-start(bf16[64,2048]{1,0:T(8,128)(2,1)} %param.11) | copy-start | bytes 786436
  73.6 44.8 %all-gather.6.cloned.1.call-start = ((), (), s32[]{:S(2)}) async-start(), calls=%async_computation.4 | async-start | bytes 1310720 | tf_op jit(solution)/shard_map/all_gather | solution.py:132
  101.6 46.3 %all-gather.8.cloned.1.call-start = ((), (), s32[]{:S(2)}) async-start(), calls=%async_computation.5 | async-start | bytes 1310720 | tf_op jit(solution)/shard_map/all_gather | solution.py:156
  102.4 77.8 %reduce-scatter.5.cloned.1.call-start = ((), (), s32[]{:S(2)}) async-start(), calls=%async_computation.6 | async-start | bytes 1310720 | tf_op jit(solution)/shard_map/reduce_scatter | solution.py:178
  121.1 1.6 collective-permute-start.5
  147.9 2.9 %copy-start.2 = (bf16[1024,2,256]{2,0,1:T(8,128)(2,1)S(1)}, bf16[1024,2,256]{2,0,1:T(8,128)(2,1)}, u32[]{:S(2)}) copy-start(bf16[1024,2,256]{2,0,1:T(8,128)(2,1)} %all-gather.8.cloned.1.call-done) | copy-start | bytes 3145732
  150.8 3.2 %copy-start.5 = (bf16[2,512,2048]{2,1,0:T(8,128)(2,1)S(1)}, bf16[2,512,2048]{2,1,0:T(8,128)(2,1)}, u32[]{:S(2)}) copy-start(bf16[2,512,2048]{2,1,0:T(8,128)(2,1)} %param.19) | copy-start | bytes 12582916
  152.0 1.8 collective-permute-start.7
  152.1 1.5 collective-permute-start.8
  152.6 1.2 collective-permute-start.6
Sparse Core Ops, SparseCore 0:
  10.5 19.4 all-gather.3
  73.7 24.5 reduce-scatter.2
  101.7 16.6 all-gather.5
  119.9 27.9 all-gather.7
  156.0 24.1 reduce-scatter.4
where the time goes:
time: 190 us
  waiting for transfers between devices  105 us (55%)
  blocking collectives  32.1 us (17%)
  matrix products  16.5 us (9%)
  between operations  15.5 us (8%)
  other arithmetic  11.6 us (6%)
  local copies, waits for them, and re-layouts  6.59 us (3%)
  starting transfers between devices  2.78 us (1%)
    reduce_scatter x2, waiting for transfers between devices, body(): lax.psum_scatter(jnp.dot(attended, out_layer, preferred_element_type=jnp....  49 us
    all_gather x2, waiting for transfers between devices, body(): lax.all_gather(normed, 'tp', axis=0, tiled=True)  27 us
    all_gather x1, waiting for transfers between devices, body(): kept_rows = lax.all_gather(later_keys, 'sp', axis=0, tiled=True)  24.9 us
    all_gather x1, blocking collectives, body(): lax.all_gather(local_keys[1], 'sp', axis=0, tiled=True)  16.1 us
    all_gather x1, blocking collectives, body(): lax.all_gather(local_keys[0], 'sp', axis=0, tiled=True)  16 us
    dot_general x2, matrix products, body(): jnp.dot(lax.all_gather(normed, 'tp', axis=0, tiled=True), layer_weight, p...  5.24 us
    reduce_sum x5, other arithmetic, rms_scaled(): jnp.mean(values * values, axis=-1, keepdims=True) + EPSILON  5.04 us
  transfers between devices with their start and end apart: 14, of which 9 were waited for; matrix products, arithmetic and copies ran while one was open for 6% of the time, Pallas kernels for 0%

commit v1 on v0

--- a/solution.py
+++ b/solution.py
@@ -153,7 +153,16 @@
                 grouped,
                 score_scale,
             )
-            kept_rows = lax.all_gather(later_keys, "sp", axis=0, tiled=True)
+            ring = [later_keys]
+            for hop in range(3):
+                ring.append(
+                    lax.ppermute(ring[-1], "sp", [(dev, (dev + 1) % 4) for dev in range(4)])
+                )
+            kept_rows = jnp.roll(
+                jnp.concatenate(ring[::-1], axis=0),
+                (lax.axis_index("sp") + 1) * ring[0].shape[0],
+                axis=0,
+            )
             row_peak, row_total, weighted, stored = updated + (kept_rows,)
         else:
             row_peak, row_total, weighted = attend(

time: 190 us -> 170 us (0.89)
  waiting for transfers between devices: 105 us -> 76 us
  local copies, waits for them, and re-layouts: 6.59 us -> 11.6 us
  starting transfers between devices: 2.78 us -> 5.35 us
    all_gather x1 -> x0, waiting for transfers between devices: 24.9 us -> none  [body(): kept_rows = lax.all_gather(later_keys, 'sp', axis=0, tiled=True)]
    ppermute x0 -> x3, waiting for transfers between devices: none -> 17 us  [body(): lax.ppermute(ring[-1], 'sp', [(dev, (dev + 1) % 4) for dev in range(4)])]
    all_gather x2, waiting for transfers between devices: 27 us -> 11.2 us  [body(): lax.all_gather(normed, 'tp', axis=0, tiled=True)]
    unnamed x17 -> x22, local copies, waits for them, and re-layouts: 0.13 us -> 5.16 us
    reduce_scatter x2, waiting for transfers between devices: 49 us -> 45.6 us  [body(): lax.psum_scatter(jnp.dot(attended, out_layer, preferred_element_type=jnp....]
    ppermute x0 -> x3, starting transfers between devices: none -> 2.65 us  [body(): lax.ppermute(ring[-1], 'sp', [(dev, (dev + 1) % 4) for dev in range(4)])]
  transfers between devices with their start and end apart: 14 -> 16, of which waited for: 9 -> 9; matrix products, arithmetic and copies ran while one was open for 6% -> 10% of each run, Pallas kernels for 0% -> 0%
where the time goes in v1:
time: 170 us
  waiting for transfers between devices  76 us (45%)
  blocking collectives  32.1 us (19%)
  matrix products  17.6 us (10%)
  between operations  15.5 us (9%)
  local copies, waits for them, and re-layouts  11.6 us (7%)
  other arithmetic  11.6 us (7%)
  starting transfers between devices  5.35 us (3%)
    reduce_scatter x2, waiting for transfers between devices, body(): lax.psum_scatter(jnp.dot(attended, out_layer, preferred_element_type=jnp....  45.6 us
    ppermute x3, waiting for transfers between devices, body(): lax.ppermute(ring[-1], 'sp', [(dev, (dev + 1) % 4) for dev in range(4)])  17 us
    all_gather x1, blocking collectives, body(): lax.all_gather(local_keys[1], 'sp', axis=0, tiled=True)  16.1 us
    all_gather x1, blocking collectives, body(): lax.all_gather(local_keys[0], 'sp', axis=0, tiled=True)  16 us
    all_gather x2, waiting for transfers between devices, body(): lax.all_gather(normed, 'tp', axis=0, tiled=True)  11.2 us
    dot_general x2, matrix products, body(): jnp.dot(lax.all_gather(normed, 'tp', axis=0, tiled=True), layer_weight, p...  5.24 us
    unnamed x22, local copies, waits for them, and re-layouts  5.16 us
    reduce_sum x5, other arithmetic, rms_scaled(): jnp.mean(values * values, axis=-1, keepdims=True) + EPSILON  5.04 us
  transfers between devices with their start and end apart: 16, of which 9 were waited for; matrix products, arithmetic and copies ran while one was open for 10% of the time, Pallas kernels for 0%

profile of v1, /device:TPU:0, one launch (start us, length us, event | category | flops | bytes accessed | tf_op | source)
XLA Modules:
  0.0 169.8 jit_solution(168338487816612429)
XLA Ops:
  7.4 1.1 fusion.51
  8.6 1.8 %fusion.53 = bf16[64,2048]{1,0:T(8,128)(2,1)} fusion(bf16[64,2048]{1,0:T(8,128)(2,1)} %param.11, f32[2048]{0:T(1024)S(1)} %bitcast.175, f32[64]{0:T(128)S(1)} %add_rsqrt_fusion.4), kind=kLoop, calls=%fused_computation.60 | loop fusion | flops 524288 | bytes 532736 | tf_op jit(solution)/shard_map/convert_element_type | solution.py:129
  10.4 2.7 %slice_bitcast_fusion.2 = (bf16[2048,128]{1,0:T(8,128)(2,1)S(1)}, bf16[2048,128]{1,0:T(8,128)(2,1)}, bf16[2048,128]{1,0:T(8,128)(2,1)}, bf16[2048,128]{1,0:T(8,128)(2,1)}) fusion(bf16[2,2048,128]{2,1,0:T(8,128)(2,1)} %param.18, bf16[2,2048,128]{2,1,0:T(8,128)(2,1)} %param.17), kind=kLoop, calls=%fused_computation.92 | loop fusion | bytes 4194304 | tf_op jit(solution)/shard_map/squeeze | solution.py:113
  13.7 2.7 %fusion.36 = bf16[512,512]{1,0:T(8,128)(2,1)S(1)} fusion(bf16[2048,128]{1,0:T(8,128)(2,1)} %get-tuple-element.28, bf16[2048,128]{1,0:T(8,128)(2,1)} %get-tuple-element.41, bf16[2048,128]{1,0:T(8,128)(2,1)S(1)} %get-tuple-element.27, bf16[2048,128]{1,0:T(8,128)(2,1)} %get-tuple-element.42, bf16[512,2048]{1,0:T(8,128)(2,1)S(1)} %copy-done.1, ...), kind=kOutput, calls=%fused_computation.41 | convolution fusion | flops 1086586880 | bytes 4728832 | tf_op jit(solution)/shard_map/dot_general | solution.py:119
  17.3 1.1 collective-permute-done.1
  18.7 11.2 %all-gather.3.cloned.1.call-done = bf16[256,2048]{1,0:T(8,128)(2,1)} async-done(((bf16[64,2048]{1,0:T(8,128)(2,1)}), bf16[256,2048]{1,0:T(8,128)(2,1)}) %all-gather.3.cloned.1.call-update) | async-done | bytes 1048592 | tf_op jit(solution)/shard_map/all_gather | solution.py:132
  30.0 2.6 %fusion.41 = bf16[256,512]{1,0:T(8,128)(2,1)S(1)} fusion(bf16[256,2048]{1,0:T(8,128)(2,1)} %all-gather.3.cloned.1.call-done, bf16[2,2048,512]{2,1,0:T(8,128)(2,1)} %param.16), kind=kOutput, calls=%fused_computation.42 | convolution fusion | flops 537001984 | bytes 3407872 | tf_op jit(solution)/shard_map/dot_general | solution.py:131
  32.9 16.0 %all_gather.13 = bf16[1024,256]{1,0:T(8,128)(2,1)S(1)} all-gather(bf16[256,256]{1,0:T(8,128)(2,1)S(1)} %bitcast.161), channel_id=1, replica_groups=mesh['grp'=2,'sp'=4,'tp'=4] {'sp'}, dimensions={0}, use_global_device_ids=true | all-gather | bytes 655360 | tf_op jit(solution)/shard_map/all_gather | solution.py:151
  49.0 16.1 %all_gather.14 = bf16[1024,256]{0,1:T(8,128)(2,1)S(1)} all-gather(bf16[256,256]{0,1:T(8,128)(2,1)S(1)} %bitcast.162), channel_id=1, replica_groups=mesh['grp'=2,'sp'=4,'tp'=4] {'sp'}, dimensions={0}, use_global_device_ids=true | all-gather | bytes 655360 | tf_op jit(solution)/shard_map/all_gather | solution.py:152
  71.7 1.8 %convolution_convert_fusion.1 = bf16[256,2048]{1,0:T(8,128)(2,1)} fusion(bf16[2,512,2048]{2,1,0:T(8,128)(2,1)S(1)} %copy-done.3, f32[256,2,512]{0,2,1:T(8,128)S(1)} %bitcast.159, s32[]{:T(128)} %bitcast.23, f32[256,2,512]{0,2,1:T(8,128)S(1)} %bitcast.158, f32[256,2,512]{0,2,1:T(8,128)S(1)} %bitcast.156, ...), kind=kOutput, calls=%fused_computation.14 | convolution fusion | flops 538574848 | bytes 5505033 | tf_op jit(solution)/shard_map/dot_general | solution.py:188
  73.7 1.1 collective-permute-start.6
  74.8 23.5 %reduce-scatter.3.cloned.1.call-done = bf16[64,2048]{1,0:T(8,128)(2,1)} async-done(((bf16[256,2048]{1,0:T(8,128)(2,1)}), bf16[64,2048]{1,0:T(8,128)(2,1)}) %reduce-scatter.3.cloned.1.call-update) | async-done | bytes 262160 | tf_op jit(solution)/shard_map/reduce_scatter | solution.py:187
  98.3 1.1 fusion.47
  99.4 1.3 fusion.55
  101.6 1.5 collective-permute-start.7
  103.2 8.2 %collective-permute-done.7 = bf16[256,2,256]{2,0,1:T(8,128)(2,1)S(1)} collective-permute-done((bf16[256,2,256]{2,0,1:T(8,128)(2,1)S(1)}, bf16[256,2,256]{2,0,1:T(8,128)(2,1)S(1)}, u32[]{:S(2)}, u32[]{:S(2)}) %collective-permute-start.7) | collective-permute-done | bytes 262176 | tf_op jit(solution)/shard_map/ppermute | solution.py:159
  111.4 8.8 %collective-permute-done.8 = bf16[256,2,256]{2,0,1:T(8,128)(2,1)S(1)} collective-permute-done((bf16[256,2,256]{2,0,1:T(8,128)(2,1)S(1)}, bf16[256,2,256]{2,0,1:T(8,128)(2,1)S(1)}, u32[]{:S(2)}, u32[]{:S(2)}) %collective-permute-start.8) | collective-permute-done | bytes 262176 | tf_op jit(solution)/shard_map/ppermute | solution.py:159
  124.5 2.6 %fusion.44 = bf16[256,512]{1,0:T(8,128)(2,1)S(1)} fusion(bf16[256,2048]{1,0:T(8,128)(2,1)} %all-gather.5.cloned.1.call-done, bf16[2,2048,512]{2,1,0:T(8,128)(2,1)} %param.16), kind=kOutput, calls=%fused_computation.43 | convolution fusion | flops 537001984 | bytes 3407872 | tf_op jit(solution)/shard_map/dot_general | solution.py:131
  129.1 1.9 %multiply_reduce_fusion = (f32[256,4]{0,1:T(4,128)S(1)}, f32[256,4,1024]{2,0,1:T(8,128)S(1)}) fusion(bf16[256,4,256]{0,2,1:T(8,128)(2,1)S(1)} %bitcast.149, bf16[2048,2,256]{2,0,1:T(8,128)(2,1)} %constant_dynamic-update-slice_fusion, s32[]{:T(128)S(6)} %select_n.87), kind=kOutput, calls=%fused_computation.7 | convolution fusion | flops 538967040 | bytes 5246980 | tf_op jit(solution)/shard_map/rhd,nd->rhn/dot_general | solution.py:78
  131.9 2.3 %fusion.7 = f32[256,4,256]{0,2,1:T(8,128)S(1)} fusion(f32[256,4,1024]{2,0,1:T(8,128)S(1)} %get-tuple-element.40, f32[256,4]{0,1:T(4,128)S(1)} %broadcast_maximum_fusion, bf16[2048,2,256]{2,0,1:T(8,128)(2,1)} %constant_dynamic-update-slice_fusion, s32[]{:T(128)S(6)} %select_n.87, s32[]{:T(128)S(6)} %add.132), kind=kOutput, calls=%fused_computation.15 | convolution fusion | flops 540016640 | bytes 5771272 | tf_op jit(solution)/shard_map/rhn,nd->rhd/dot_general | solution.py:84
  136.3 1.8 %convolution_convert_fusion = bf16[256,2048]{1,0:T(8,128)(2,1)} fusion(bf16[2,512,2048]{2,1,0:T(8,128)(2,1)S(1)} %copy-done.4, f32[256,2,512]{0,2,1:T(8,128)S(1)} %bitcast.157, s32[]{:T(128)} %bitcast.23, f32[256,2,512]{0,2,1:T(8,128)S(1)} %bitcast.155, f32[256,2,512]{0,2,1:T(8,128)S(1)} %bitcast.154, bf16[256,1,512]{0,2,1:T(8,128)(2,1)S(1)} %collective-permute-done.10, ...), kind=kOutput, calls=%fused_computation.13 | convolution fusion | flops 538574848 | bytes 5505033 | tf_op jit(solution)/shard_map/dot_general | solution.py:188
  138.2 22.2 %reduce-scatter.5.cloned.1.call-done = bf16[64,2048]{1,0:T(8,128)(2,1)} async-done(((bf16[256,2048]{1,0:T(8,128)(2,1)}), bf16[64,2048]{1,0:T(8,128)(2,1)}) %reduce-scatter.5.cloned.1.call-update) | async-done | bytes 262160 | tf_op jit(solution)/shard_map/reduce_scatter | solution.py:187
  160.4 1.1 fusion.49
  161.5 1.8 %fusion.58 = bf16[64,2048]{1,0:T(8,128)(2,1)} fusion(bf16[64,2048]{1,0:T(8,128)(2,1)} %reduce-scatter.5.cloned.1.call-done, bf16[64,2048]{1,0:T(8,128)(2,1)S(1)} %get-tuple-element.21, f32[2048]{0:T(1024)S(1)} %bitcast.173, f32[64]{0:T(128)S(1)} %add_rsqrt_fusion.1), kind=kLoop, calls=%fused_computation.65 | loop fusion | flops 786432 | bytes 794880 | tf_op jit(solution)/shard_map/convert_element_type | solution.py:195
  (93 shorter events, 17.9 us)
Async XLA Ops:
  6.5 6.6 %copy-start.1 = (bf16[512,2048]{1,0:T(8,128)(2,1)S(1)}, bf16[512,2048]{1,0:T(8,128)(2,1)}, u32[]{:S(2)}) copy-start(bf16[512,2048]{1,0:T(8,128)(2,1)} %param.12) | copy-start | bytes 6291460
  6.5 7.2 %copy-start.5 = (f32[2048]{0:T(1024)S(1)}, f32[2048]{0:T(1024)}, u32[]{:S(2)}) copy-start(f32[2048]{0:T(1024)} %param.13) | copy-start | bytes 24580
  6.5 23.4 %all-gather.3.cloned.1.call-start = ((), (), s32[]{:S(2)}) async-start(), calls=%async_computation.2 | async-start | bytes 1310720 | tf_op jit(solution)/shard_map/all_gather | solution.py:132
  10.4 87.9 %reduce-scatter.3.cloned.1.call-start = ((), (), s32[]{:S(2)}) async-start(), calls=%async_computation.3 | async-start | bytes 1310720 | tf_op jit(solution)/shard_map/reduce_scatter | solution.py:187
  16.7 1.7 %collective-permute-start.1 = (bf16[1,1,256,4,128]{4,2,3,1,0:T(8,128)(2,1)S(1)}, bf16[1,1,256,4,128]{4,2,3,1,0:T(8,128)(2,1)S(1)}, u32[]{:S(2)}, u32[]{:S(2)}) collective-permute-start(bf16[1,1,256,4,128]{4,2,3,1,0:T(8,128)(2,1)S(1)} %bitcast.164), channel_id=1, source_target_pairs={{0,1},{1,0},{2,3},{3,2},{4,5},{5,4},{6,7},{7,6},{8,9},{9,8},{10,11... | collective-permute-start | bytes 786440 | tf_op jit(solution)/shard_map/ppermute | solution.py:16
  32.6 32.5 %collective-permute-start = (bf16[1,1,256,512]{3,2,1,0:T(8,128)(2,1)S(1)}, bf16[1,1,256,512]{3,2,1,0:T(8,128)(2,1)S(1)}, u32[]{:S(2)}, u32[]{:S(2)}) collective-permute-start(bf16[1,1,256,512]{3,2,1,0:T(8,128)(2,1)S(1)} %bitcast.165), channel_id=1, source_target_pairs={{0,1},{1,0},{2,3},{3,2},{4,5},{5,4},{6,7},{7,6},{8,9},{9,8},{10,11... | collective-permute-start | bytes 786440 | tf_op jit(solution)/shard_map/ppermute | solution.py:16
  67.2 4.6 %copy-start.3 = (bf16[2,512,2048]{2,1,0:T(8,128)(2,1)S(1)}, bf16[2,512,2048]{2,1,0:T(8,128)(2,1)}, u32[]{:S(2)}) copy-start(bf16[2,512,2048]{2,1,0:T(8,128)(2,1)} %param.19) | copy-start | bytes 12582916
  68.2 3.3 %collective-permute-start.3 = (bf16[256,1,512]{0,2,1:T(8,128)(2,1)S(1)}, bf16[256,1,512]{0,2,1:T(8,128)(2,1)S(1)}, u32[]{:S(2)}, u32[]{:S(2)}) collective-permute-start(bf16[256,1,512]{0,2,1:T(8,128)(2,1)S(1)} %fusion.72), channel_id=1, source_target_pairs={{0,1},{1,0},{2,3},{3,2},{4,5},{5,4},{6,7},{7,6},{8,9},{9,8},{10,11... | collective-permute-start | bytes 786440 | tf_op jit(solution)/shard_map/ppermute | solution.py:16
  68.3 3.1 %collective-permute-start.4 = (bf16[256,4]{0,1:T(4,128)(2,1)S(1)}, bf16[256,4]{0,1:T(4,128)(2,1)S(1)}, u32[]{:S(2)}, u32[]{:S(2)}) collective-permute-start(bf16[256,4]{0,1:T(4,128)(2,1)S(1)} %convert_element_type.135), channel_id=1, source_target_pairs={{0,1},{1,0},{2,3},{3,2},{4,5},{5,4},{6,7},{7,6},{8,9},{9,8},{10,11... | collective-permute-start | bytes 6152 | tf_op jit(solution)/shard_map/ppermute | solution.py:16
  68.8 2.6 %collective-permute-start.2 = (bf16[256,4]{0,1:T(4,128)(2,1)S(1)}, bf16[256,4]{0,1:T(4,128)(2,1)S(1)}, u32[]{:S(2)}, u32[]{:S(2)}) collective-permute-start(bf16[256,4]{0,1:T(4,128)(2,1)S(1)} %fusion.93), channel_id=1, source_target_pairs={{0,1},{1,0},{2,3},{3,2},{4,5},{5,4},{6,7},{7,6},{8,9},{9,8},{10,11... | collective-permute-start | bytes 6152 | tf_op jit(solution)/shard_map/ppermute | solution.py:16
  71.6 2.0 %copy-start.2 = (f32[2,2048]{1,0:T(2,128)S(1)}, f32[2,2048]{1,0:T(2,128)}, u32[]{:S(2)}) copy-start(f32[2,2048]{1,0:T(2,128)} %param.15) | copy-start | bytes 49156
  71.7 27.7 %copy-start = (bf16[64,2048]{1,0:T(8,128)(2,1)S(1)}, bf16[64,2048]{1,0:T(8,128)(2,1)}, u32[]{:S(2)}) copy-start(bf16[64,2048]{1,0:T(8,128)(2,1)} %param.11) | copy-start | bytes 786436
  73.6 50.9 %all-gather.5.cloned.1.call-start = ((), (), s32[]{:S(2)}) async-start(), calls=%async_computation.4 | async-start | bytes 1310720 | tf_op jit(solution)/shard_map/all_gather | solution.py:132
  73.7 27.9 %collective-permute-start.6 = (bf16[256,2,256]{2,0,1:T(8,128)(2,1)S(1)}, bf16[256,2,256]{2,0,1:T(8,128)(2,1)S(1)}, u32[]{:S(2)}, u32[]{:S(2)}) collective-permute-start(bf16[256,2,256]{2,0,1:T(8,128)(2,1)S(1)} %bitcast_bitcast_fusion), channel_id=1, source_target_pairs={{0,4},{4,8},{8,12},{12,0},{1,5},{5,9},{9,13},{13,1},{2,6},{6,10},{... | collective-permute-start | bytes 786440 | tf_op jit(solution)/shard_map/ppermute | solution.py:159
  101.6 58.8 %reduce-scatter.5.cloned.1.call-start = ((), (), s32[]{:S(2)}) async-start(), calls=%async_computation.5 | async-start | bytes 1310720 | tf_op jit(solution)/shard_map/reduce_scatter | solution.py:187
  101.6 9.8 %collective-permute-start.7 = (bf16[256,2,256]{2,0,1:T(8,128)(2,1)S(1)}, bf16[256,2,256]{2,0,1:T(8,128)(2,1)S(1)}, u32[]{:S(2)}, u32[]{:S(2)}) collective-permute-start(bf16[256,2,256]{2,0,1:T(8,128)(2,1)S(1)} %collective-permute-done.6), channel_id=1, source_target_pairs={{0,4},{4,8},{8,12},{12,0},{1,5},{5,9},{9,13},{13,1},{2,6},{6,10},{... | collective-permute-start | bytes 786440 | tf_op jit(solution)/shard_map/ppermute | solution.py:159
  111.4 8.8 %collective-permute-start.8 = (bf16[256,2,256]{2,0,1:T(8,128)(2,1)S(1)}, bf16[256,2,256]{2,0,1:T(8,128)(2,1)S(1)}, u32[]{:S(2)}, u32[]{:S(2)}) collective-permute-start(bf16[256,2,256]{2,0,1:T(8,128)(2,1)S(1)} %collective-permute-done.7), channel_id=1, source_target_pairs={{0,4},{4,8},{8,12},{12,0},{1,5},{5,9},{9,13},{13,1},{2,6},{6,10},{... | collective-permute-start | bytes 786440 | tf_op jit(solution)/shard_map/ppermute | solution.py:159
  127.2 1.6 collective-permute-start.5
  131.9 4.5 %copy-start.4 = (bf16[2,512,2048]{2,1,0:T(8,128)(2,1)S(1)}, bf16[2,512,2048]{2,1,0:T(8,128)(2,1)}, u32[]{:S(2)}) copy-start(bf16[2,512,2048]{2,1,0:T(8,128)(2,1)} %param.19) | copy-start | bytes 12582916
  134.2 1.9 %collective-permute-start.10 = (bf16[256,1,512]{0,2,1:T(8,128)(2,1)S(1)}, bf16[256,1,512]{0,2,1:T(8,128)(2,1)S(1)}, u32[]{:S(2)}, u32[]{:S(2)}) collective-permute-start(bf16[256,1,512]{0,2,1:T(8,128)(2,1)S(1)} %fusion.73), channel_id=1, source_target_pairs={{0,1},{1,0},{2,3},{3,2},{4,5},{5,4},{6,7},{7,6},{8,9},{9,8},{10,11... | collective-permute-start | bytes 786440 | tf_op jit(solution)/shard_map/ppermute | solution.py:16
  134.7 1.2 collective-permute-start.11
  134.8 1.2 collective-permute-start.9
Sparse Core Ops, SparseCore 0:
  10.5 19.4 all-gather.2
  73.7 24.5 reduce-scatter.2
  101.7 16.6 all-gather.4
  138.3 22.0 reduce-scatter.4
